TPU v7x, 32 devices: a whole 2x2x4 slice. The times are simulated.
32 devices in a mesh: sp: 8 (over z, x), tp: 4 (over y, core).
Axes of the slice: x: 2, y: 2, z: 4, core: 2. Of those that a mesh axis runs over, the one named last changes fastest.
Arguments:
- resid: bfloat16 [2048, 4096], P(('sp', 'tp')), may hold values from -6 to 6
- queries: bfloat16 [2048, 2048], P('sp', 'tp'), may hold values from -6 to 6
- keys: bfloat16 [2048, 512], P('sp', 'tp'), may hold values from -6 to 6
- values: bfloat16 [2048, 512], P('sp', 'tp'), may hold values from -6 to 6
- q_gain: float32 [128], replicated, may hold values from 0.5 to 6
- key_norm_gain: float32 [128], replicated, may hold values from 0.5 to 6
- out_weight: bfloat16 [2048, 4096], P('tp'), may hold values from -0.125 to 0.125
- norm1_gain: float32 [4096], replicated, may hold values from 0.1 to 1.9
- norm2_gain: float32 [4096], replicated, may hold values from 0.1 to 1.9
- expert_ids: int32 [2048, 2], P(('sp', 'tp')), may hold values from 0 to 7, all different within a row; in each aligned block of 64 rows (0 to 63, 64 to 127, ...) at most 24 rows name the same one
- group_weight: float32 [2048], P(('sp', 'tp')), may hold values from 0.3 to 1
- expert_weight: float32 [2048, 2], P(('sp', 'tp')), may hold values from 0.1 to 1
- gate_proj: bfloat16 [8, 4096, 1024], P('sp', None, 'tp'), may hold values from -0.09375 to 0.09375
- up_proj: bfloat16 [8, 4096, 1024], P('sp', None, 'tp'), may hold values from -0.09375 to 0.09375
- down_proj: bfloat16 [8, 1024, 4096], P('sp', 'tp'), may hold values from -0.1875 to 0.1875
Outputs:
- mixed_out: bfloat16 [2048, 4096], P(('sp', 'tp'))
Inputs may be any that keep to these rules, and one draw needn't show every extreme that they name: `expert_ids`: each row names 2 different experts. Among the rows of one device (aligned blocks of 64 rows) no expert is named by more than 24 rows, a bound that some block reaches.
All inputs are finite; a program needn't handle non-finite values.
Results may differ from a plain program's by a relative error of at most 0.012.
The roundings to bfloat16 on the way count: a program that leaves them out, or rounds other values in their place, can miss the bound.
Values may be sent and summed in bfloat16 or wider, within the bound.
A program may use at most 192 MiB of HBM per device.

v0:
```python
import math

import jax
import jax.numpy as jnp
from jax import lax
from jax.sharding import PartitionSpec as P

GRID_W = 64


deep_alpha = 2.0**0.5
rope_theta = 10000.0


def apply_rotary_heads(block, gain, grid_positions):
    values32 = block.astype(jnp.float32)
    normed = values32 * lax.rsqrt(jnp.mean(values32 * values32, -1, keepdims=True) + 1e-06) * gain
    half = normed.shape[-1] // 2
    inv_freq = rope_theta ** (-jnp.arange(0, half, 2, dtype=jnp.float32) / half)
    grid_row = (grid_positions // GRID_W).astype(jnp.float32)
    grid_col = (grid_positions % GRID_W).astype(jnp.float32)
    angle = jnp.concatenate([grid_row[:, None] * inv_freq, grid_col[:, None] * inv_freq], -1)[
        :, None, :
    ]
    cosine = jnp.cos(angle)
    sine = jnp.sin(angle)
    first = normed[..., :half]
    second = normed[..., half:]
    turned = jnp.concatenate([first * cosine - second * sine, first * sine + second * cosine], -1)
    return turned.astype(jnp.bfloat16)


def layer_norm_gain(summed, gain):
    centre = summed - jnp.mean(summed, -1, keepdims=True)
    spread = jnp.mean(centre * centre, -1, keepdims=True)
    return centre * lax.rsqrt(spread + 1e-06) * gain


def per_device(
    resid,
    queries,
    keys,
    values,
    q_gain,
    key_norm_gain,
    out_weight,
    norm1_gain,
    norm2_gain,
    expert_ids,
    group_weight,
    expert_weight,
    gate_proj,
    up_proj,
    down_proj,
):
    local_tokens = queries.shape[0]
    head_size = q_gain.shape[0]
    kv_local = keys.shape[1] // head_size
    query_group = queries.shape[1] // head_size // kv_local
    model_width = resid.shape[1]
    score_scale = head_size ** (-0.5)
    grid_positions = lax.axis_index("sp") * local_tokens + jnp.arange(local_tokens, dtype=jnp.int32)
    q_rot = apply_rotary_heads(
        queries.reshape(local_tokens, kv_local * query_group, head_size), q_gain, grid_positions
    )
    query_head_rows = q_rot.reshape(local_tokens, kv_local, query_group, head_size).transpose(
        1, 2, 0, 3
    )
    query_head_rows = query_head_rows.reshape(kv_local, query_group * local_tokens, head_size)
    rotated_keys = apply_rotary_heads(
        keys.reshape(local_tokens, kv_local, head_size), key_norm_gain, grid_positions
    )
    rotated_keys = rotated_keys.reshape(local_tokens, kv_local * head_size)
    start_state = (
        jnp.full((kv_local, query_group * local_tokens), -1e30, jnp.float32),
        jnp.zeros((kv_local, query_group * local_tokens), jnp.float32),
        jnp.zeros((kv_local, query_group * local_tokens, head_size), jnp.float32),
    )
    key_piece = lax.all_gather(rotated_keys, "sp", axis=0, tiled=True)
    value_piece = lax.all_gather(values, "sp", axis=0, tiled=True)
    length = key_piece.shape[0]
    span = math.gcd(length, 512)
    key_blocks = key_piece.reshape(length // span, span, kv_local, head_size)
    value_blocks = value_piece.reshape(length // span, span, kv_local, head_size)

    def inner(state, blocks):
        row_max, row_sum, weighted = state
        key_tile, value_block = blocks
        scores = (
            jnp.einsum(
                "pmw,fpw->pmf", query_head_rows, key_tile, preferred_element_type=jnp.float32
            )
            * score_scale
        )
        new_max = jnp.maximum(row_max, jnp.max(scores, -1))
        shrink_old = jnp.exp(row_max - new_max)
        probs = jnp.exp(scores - new_max[..., None])
        row_sum = row_sum * shrink_old + jnp.sum(probs, -1)
        weighted = weighted * shrink_old[..., None] + jnp.einsum(
            "wno,ows->wns",
            probs.astype(jnp.bfloat16),
            value_block,
            preferred_element_type=jnp.float32,
        )
        return ((new_max, row_sum, weighted), None)

    state, _ = lax.scan(inner, start_state, (key_blocks, value_blocks))
    row_max, row_sum, weighted = state
    attn = (weighted / row_sum[..., None]).astype(jnp.bfloat16)
    attn = attn.reshape(kv_local, query_group, local_tokens, head_size).transpose(2, 0, 1, 3)
    attn = attn.reshape(local_tokens, kv_local * query_group * head_size)
    lanes = lax.axis_size("tp")
    own_rows = local_tokens // lanes
    merged = lax.all_to_all(attn, "tp", split_axis=0, concat_axis=1, tiled=True)
    proj = jnp.dot(
        merged,
        lax.all_gather(out_weight, "tp", axis=0, tiled=True),
        preferred_element_type=jnp.float32,
    )
    proj = proj.astype(jnp.bfloat16)
    summed = deep_alpha * resid.astype(jnp.float32) + proj.astype(jnp.float32)
    x_one = layer_norm_gain(summed, norm1_gain).astype(jnp.bfloat16)
    top_count = expert_ids.shape[1]
    sp_count = lax.axis_size("sp")
    expert_local = gate_proj.shape[0]
    expert_total = expert_local * sp_count
    capacity = (3 * top_count * own_rows + 2 * expert_total - 1) // (2 * expert_total)
    flat_ids = expert_ids.reshape(-1)
    one_hot = (flat_ids[:, None] == jnp.arange(expert_total, dtype=jnp.int32)[None, :]).astype(
        jnp.int32
    )
    earlier = jnp.cumsum(one_hot, 0) - one_hot
    rank = jnp.sum(earlier * one_hot, 1)
    slot = flat_ids * capacity + rank
    placing = slot[:, None] == jnp.arange(expert_total * capacity, dtype=jnp.int32)[None, :]
    placing = placing.astype(jnp.bfloat16).reshape(own_rows, top_count, expert_total * capacity)
    placing = jnp.sum(placing, 1)
    outgoing = lax.dot_general(
        placing, x_one, (((0,), (0,)), ((), ())), preferred_element_type=jnp.float32
    ).astype(jnp.bfloat16)
    outgoing = outgoing.reshape(expert_total, capacity, model_width)
    received = lax.all_to_all(outgoing, "sp", split_axis=0, concat_axis=0, tiled=True)
    arrived = received.reshape(sp_count, expert_local, capacity, model_width).transpose(0, 2, 1, 3)
    arrived = arrived.reshape(sp_count * capacity, expert_local, model_width)
    piece = lax.all_gather(arrived, "tp", axis=0, tiled=True)
    gate_part = jnp.einsum("red,edf->ref", piece, gate_proj, preferred_element_type=jnp.float32)
    up_part = jnp.einsum("red,edf->ref", piece, up_proj, preferred_element_type=jnp.float32)
    hidden = (jax.nn.silu(gate_part) * up_part).astype(jnp.bfloat16)
    partial_sum = jnp.einsum("ref,efd->red", hidden, down_proj, preferred_element_type=jnp.float32)
    rounded = lax.optimization_barrier(partial_sum.astype(jnp.bfloat16))
    expert_out = lax.psum_scatter(
        rounded.astype(jnp.float32).astype(jnp.bfloat16), "tp", scatter_dimension=0, tiled=True
    )
    returning = expert_out.reshape(sp_count, capacity, expert_local, model_width).transpose(
        0, 2, 1, 3
    )
    returning = returning.reshape(sp_count * expert_local, capacity, model_width)
    returned = lax.all_to_all(returning, "sp", split_axis=0, concat_axis=0, tiled=True)
    returned = returned.reshape(expert_total * capacity, model_width)
    picked_out = returned[slot].reshape(own_rows, top_count, model_width)
    gates = group_weight[:, None] * expert_weight / jnp.sum(expert_weight, -1, keepdims=True)
    moe = jnp.sum(gates[..., None] * picked_out.astype(jnp.float32), 1)
    final = deep_alpha * x_one.astype(jnp.float32) + moe
    return layer_norm_gain(final, norm2_gain).astype(jnp.bfloat16)


def solution(mesh):
    in_specs = (
        P(("sp", "tp"), None),
        P("sp", "tp"),
        P("sp", "tp"),
        P("sp", "tp"),
        P(),
        P(),
        P("tp", None),
        P(),
        P(),
        P(("sp", "tp"), None),
        P(("sp", "tp")),
        P(("sp", "tp"), None),
        P("sp", None, "tp"),
        P("sp", None, "tp"),
        P("sp", "tp", None),
    )
    out_specs = P(("sp", "tp"), None)
    return jax.shard_map(
        per_device, mesh=mesh, in_specs=in_specs, out_specs=out_specs, check_vma=False
    )
```

profile of v0, /device:TPU:0, one launch (start us, length us, event | category | flops | bytes accessed | tf_op | source)
XLA Modules:
  0.0 359.7 jit_solution(5686373817710456850)
XLA Ops:
  11.2 33.0 %all_gather.12 = bf16[2048,128]{1,0:T(8,128)(2,1)S(1)} all-gather(bf16[256,128]{1,0:T(8,128)(2,1)S(1)} %pad_maximum_fusion.2), channel_id=1, replica_groups=mesh['sp'=8,'tp'=4] {'sp'}, dimensions={0}, use_global_device_ids=true | all-gather | bytes 589824 | tf_op jit(solution)/shard_map/all_gather | solution.py:79
  44.2 33.3 %all_gather.13 = bf16[2048,128]{1,0:T(8,128)(2,1)} all-gather(bf16[256,128]{1,0:T(8,128)(2,1)S(1)} %copy-done.5), channel_id=1, replica_groups=mesh['sp'=8,'tp'=4] {'sp'}, dimensions={0}, use_global_device_ids=true | all-gather | bytes 589824 | tf_op jit(solution)/shard_map/all_gather | solution.py:80
  77.5 22.3 %while.15 = (s32[]{:T(128)}, f32[1,1024]{1,0:T(1,128)S(1)}, f32[1,1024]{1,0:T(1,128)S(1)}, f32[1,1024,128]{2,1,0:T(8,128)S(1)}, bf16[4,512,1,128]{3,1,2,0:T(8,12...) while((s32[]{:T(128)}, f32[1,1024]{1,0:T(1,128)S(1)}, ...), condition=%wide.region_5.6_spmd.clone, body=%wide.region_2.5_spmd.clone.sunk | while | flops 273028096 | bytes 16319113 | solution.py:107
  79.3 2.1 fusion.98
  83.1 1.8 multiply_reduce_fusion.6
  84.9 2.1 fusion.98
  88.6 1.8 multiply_reduce_fusion.6
  90.4 2.1 fusion.98
  94.2 1.8 multiply_reduce_fusion.6
  96.0 2.1 fusion.98
  101.0 3.4 all-to-all-start
  105.5 8.1 %all-to-all-done = bf16[4,64,512]{2,1,0:T(8,128)(2,1)S(1)} async-done(((bf16[4,64,512]{2,1,0:T(8,128)(2,1)}), bf16[4,64,512]{2,1,0:T(8,128)(2,1)S(1)}, u32[]{:S(2)}, u32[]{:S(2)}) %all-to-all-start) | async-done | bytes 262176 | tf_op jit(solution)/shard_map/all_to_all | solution.py:114
  113.7 6.7 %all-gather.3.cloned.1.call-done = bf16[2048,4096]{1,0:T(8,128)(2,1)} async-done(((bf16[512,4096]{1,0:T(8,128)(2,1)}), bf16[2048,4096]{1,0:T(8,128)(2,1)}) %all-gather.3.cloned.1.call-update) | async-done | bytes 16777232 | tf_op jit(solution)/shard_map/all_gather | solution.py:117
  120.4 9.0 %fusion.84 = (f32[64]{0:T(128)S(1)}, f32[64,4096]{1,0:T(8,128)S(1)}) fusion(bf16[64,2048]{1,0:T(8,128)(2,1)S(1)} %bitcast.160, bf16[2048,4096]{1,0:T(8,128)(2,1)} %all-gather.3.cloned.1.call-done, bf16[64,4096]{1,0:T(8,128)(2,1)} %param.17), kind=kOutput, calls=%fused_computation.114 | convolution fusion | flops 1075314688 | bytes 18612480 | tf_op jit(solution)/shard_map/dot_general | solution.py:115
  130.3 42.8 %all_to_all.29 = bf16[8,24,4096]{2,1,0:T(8,128)(2,1)} all-to-all(bf16[8,24,4096]{2,1,0:T(8,128)(2,1)S(1)} %bitcast.154), channel_id=1, replica_groups=mesh['sp'=8,'tp'=4] {'sp'}, dimensions={0} | all-to-all | bytes 3145728 | tf_op jit(solution)/shard_map/all_to_all | solution.py:142
  173.3 44.4 %all-gather.5.cloned.1.call-done = bf16[768,1,4096]{2,0,1:T(8,128)(2,1)} async-done(((bf16[192,1,4096]{2,0,1:T(8,128)(2,1)}), bf16[768,1,4096]{2,0,1:T(8,128)(2,1)}) %all-gather.5.cloned.1.call-update) | async-done | bytes 6291472 | tf_op jit(solution)/shard_map/all_gather | solution.py:145
  217.7 6.1 %fusion.28 = f32[768,1,256]{2,0,1:T(8,128)} fusion(bf16[1,4096,256]{2,1,0:T(8,128)(2,1)} %param.29, bf16[768,1,4096]{2,0,1:T(8,128)(2,1)} %all-gather.5.cloned.1.call-done), kind=kOutput, calls=%fused_computation.39 | convolution fusion | flops 1610612736 | bytes 9175040 | tf_op jit(solution)/shard_map/red,edf->ref/dot_general | solution.py:146
  223.9 12.8 %fusion.22 = bf16[768,1,4096]{2,0,1:T(8,128)(2,1)} fusion(bf16[1,256,4096]{2,1,0:T(8,128)(2,1)S(1)} %copy-done, bf16[1,4096,256]{2,1,0:T(8,128)(2,1)} %param.30, bf16[768,1,4096]{2,0,1:T(8,128)(2,1)} %all-gather.5.cloned.1.call-done, f32[768,1,256]{2,0,1:T(8,128)} %fusion.28), kind=kOutput, calls=%fused_computation.30 | convolution fusion | flops 3225550848 | bytes 17563648 | tf_op jit(solution)/shard_map/ref,efd->red/dot_general | solution.py:149
  236.7 59.0 %reduce-scatter.2.cloned.1.call-done = bf16[192,1,4096]{2,0,1:T(8,128)(2,1)} async-done(((bf16[768,1,4096]{2,0,1:T(8,128)(2,1)}), bf16[192,1,4096]{2,0,1:T(8,128)(2,1)}) %reduce-scatter.2.cloned.1.call-update) | async-done | bytes 1572880 | tf_op jit(solution)/shard_map/reduce_scatter | solution.py:151
  295.7 5.5 %all-to-all-start.2 = ((bf16[8,24,4096]{2,1,0:T(8,128)(2,1)}), bf16[8,24,4096]{2,1,0:T(8,128)(2,1)}, u32[]{:S(2)}, u32[]{:S(2)}) async-start(bf16[8,24,4096]{2,1,0:T(8,128)(2,1)} %bitcast.159), calls=%async_computation.3 | async-start | bytes 3145728 | tf_op jit(solution)/shard_map/all_to_all | solution.py:158
  301.5 36.6 %all-to-all-done.2 = bf16[8,24,4096]{2,1,0:T(8,128)(2,1)} async-done(((bf16[8,24,4096]{2,1,0:T(8,128)(2,1)}), bf16[8,24,4096]{2,1,0:T(8,128)(2,1)}, u32[]{:S(2)}, u32[]{:S(2)}) %all-to-all-start.2) | async-done | bytes 1572896 | tf_op jit(solution)/shard_map/all_to_all | solution.py:158
  338.1 4.8 %gather_fusion = bf16[128,4096]{1,0:T(8,128)(2,1)} fusion(bf16[192,4096]{1,0:T(8,128)(2,1)} %bitcast.36, s32[1024]{0:T(1024)S(1)} %pad_clamp_fusion), kind=kCustom, calls=%fused_computation | custom fusion | bytes 2097664 | tf_op jit(solution)/shard_map/gather | solution.py:160
  342.9 3.4 reshape.421
  346.3 4.8 %multiply_reduce_fusion.1 = f32[64,4096]{1,0:T(8,128)S(1)} fusion(f32[64,2,4096]{2,1,0:T(2,128)} %reshape.421, f32[64,2]{1,0:T(8,128)S(1)} %copy.52), kind=kLoop, calls=%fused_computation.38 | loop fusion | flops 786432 | bytes 3146240 | tf_op jit(solution)/shard_map/reduce_sum | solution.py:162
  (100 shorter events, 18.6 us)
Async XLA Ops:
  6.5 217.3 %copy-start = (bf16[1,256,4096]{2,1,0:T(8,128)(2,1)S(1)}, bf16[1,256,4096]{2,1,0:T(8,128)(2,1)}, u32[]{:S(2)}) copy-start(bf16[1,256,4096]{2,1,0:T(8,128)(2,1)} %param.31) | copy-start | bytes 6291460
  6.5 1.1 copy-start.3
  6.5 113.8 %all-gather.3.cloned.1.call-start = ((), (), s32[]{:S(2)}) async-start(), calls=%async_computation.4 | async-start | bytes 20971520 | tf_op jit(solution)/shard_map/all_gather | solution.py:117
  7.3 1.7 copy-start.9
  8.9 1.3 copy-start.4
  8.9 1.4 copy-start.10
  9.3 34.9 %copy-start.5 = (bf16[256,128]{1,0:T(8,128)(2,1)S(1)}, bf16[256,128]{1,0:T(8,128)(2,1)}, u32[]{:S(2)}) copy-start(bf16[256,128]{1,0:T(8,128)(2,1)} %param.20) | copy-start | bytes 196612
  79.3 2.2 copy-start.1
  84.8 2.2 copy-start.1
  90.4 2.2 copy-start.1
  96.0 2.2 copy-start.1
  99.8 4.7 %copy-start.8 = (s32[64,2]{0,1:T(2,128)S(1)}, s32[64,2]{0,1:T(2,128)}, u32[]{:S(2)}) copy-start(s32[64,2]{0,1:T(2,128)} %param.26) | copy-start | bytes 1540
  101.0 12.6 %all-to-all-start = ((bf16[4,64,512]{2,1,0:T(8,128)(2,1)}), bf16[4,64,512]{2,1,0:T(8,128)(2,1)S(1)}, u32[]{:S(2)}, u32[]{:S(2)}) async-start(bf16[4,64,512]{2,1,0:T(8,128)(2,1)} %all_to_all.20), calls=%async_computation | async-start | bytes 524288 | tf_op jit(solution)/shard_map/all_to_all | solution.py:114
  104.4 113.3 %all-gather.5.cloned.1.call-start = ((), (), s32[]{:S(2)}) async-start(), calls=%async_computation.5 | async-start | bytes 7864320 | tf_op jit(solution)/shard_map/all_gather | solution.py:145
  120.4 9.3 %copy-start.2 = (f32[4096]{0:T(1024)S(1)}, f32[4096]{0:T(1024)}, u32[]{:S(2)}) copy-start(f32[4096]{0:T(1024)} %param.24) | copy-start | bytes 49156
  173.1 122.6 %reduce-scatter.2.cloned.1.call-start = ((), (), s32[]{:S(2)}) async-start(), calls=%async_computation.6 | async-start | bytes 7864320 | tf_op jit(solution)/shard_map/reduce_scatter | solution.py:151
  236.7 64.6 %copy-start.7 = (f32[64,2]{0,1:T(2,128)S(1)}, f32[64,2]{0,1:T(2,128)}, u32[]{:S(2)}) copy-start(f32[64,2]{0,1:T(2,128)} %param.28) | copy-start | bytes 1540
  236.7 64.7 %copy-start.11 = (f32[64]{0:T(128)S(1)}, f32[64]{0:T(128)}, u32[]{:S(2)}) copy-start(f32[64]{0:T(128)} %param.27) | copy-start | bytes 772
  295.7 42.4 %all-to-all-start.2 = ((bf16[8,24,4096]{2,1,0:T(8,128)(2,1)}), bf16[8,24,4096]{2,1,0:T(8,128)(2,1)}, u32[]{:S(2)}, u32[]{:S(2)}) async-start(bf16[8,24,4096]{2,1,0:T(8,128)(2,1)} %bitcast.159), calls=%async_computation.3 | async-start | bytes 3145728 | tf_op jit(solution)/shard_map/all_to_all | solution.py:158
  351.1 0.9 copy-start.6
Sparse Core Ops, SparseCore 0:
  8.9 111.4 all-gather.2
  173.2 44.4 all-gather.4
  236.8 58.8 reduce-scatter.1
where the time goes:
time: 360 us
  waiting for transfers between devices  156 us (43%)
  blocking collectives  109 us (30%)
  matrix products  41.8 us (12%)
  other arithmetic  19.7 us (5%)
  between operations  13.5 us (4%)
  local copies, waits for them, and re-layouts  10.8 us (3%)
  starting transfers between devices  9.18 us (3%)
    reduce_scatter x1, waiting for transfers between devices, per_device(): lax.psum_scatter(rounded.astype(jnp.float32).astype(jnp.bfloat16), 'tp',...  59 us
    all_gather x1, waiting for transfers between devices, per_device(): piece = lax.all_gather(arrived, 'tp', axis=0, tiled=True)  44.4 us
    all_to_all x1, blocking collectives, per_device(): lax.all_to_all(outgoing, 'sp', split_axis=0, concat_axis=0, tiled=True)  42.8 us
    all_to_all x1, waiting for transfers between devices, per_device(): lax.all_to_all(returning, 'sp', split_axis=0, concat_axis=0, tiled=True)  36.6 us
    all_gather x1, blocking collectives, per_device(): value_piece = lax.all_gather(values, 'sp', axis=0, tiled=True)  33.3 us
    all_gather x1, blocking collectives, per_device(): key_piece = lax.all_gather(rotated_keys, 'sp', axis=0, tiled=True)  33 us
    dot_general x1, matrix products, per_device(): jnp.einsum('ref,efd->red', hidden, down_proj, preferred_element_type=jnp....  12.8 us
    dot_general x1, matrix products, per_device(): jnp.dot(merged, lax.all_gather(out_weight, 'tp', axis=0, tiled=True), pre...  8.95 us
  transfers between devices with their start and end apart: 5, of which 5 were waited for; matrix products, arithmetic and copies ran while one was open for 7% of the time, Pallas kernels for 0%

commit v1 on v0

v1 whole, which is shorter than its diff:
```python
import functools

import jax
import jax.numpy as jnp
from jax import lax
from jax.experimental import pallas as pl
from jax.experimental.pallas import tpu as pltpu
from jax.sharding import PartitionSpec as P

GRID_W = 64


deep_alpha = 2.0**0.5
rope_theta = 10000.0


def apply_rotary_heads(block, gain, grid_positions):
    values32 = block.astype(jnp.float32)
    normed = values32 * lax.rsqrt(jnp.mean(values32 * values32, -1, keepdims=True) + 1e-06) * gain
    half = normed.shape[-1] // 2
    inv_freq = rope_theta ** (-jnp.arange(0, half, 2, dtype=jnp.float32) / half)
    grid_row = (grid_positions // GRID_W).astype(jnp.float32)
    grid_col = (grid_positions % GRID_W).astype(jnp.float32)
    angle = jnp.concatenate([grid_row[:, None] * inv_freq, grid_col[:, None] * inv_freq], -1)[
        :, None, :
    ]
    cosine = jnp.cos(angle)
    sine = jnp.sin(angle)
    first = normed[..., :half]
    second = normed[..., half:]
    turned = jnp.concatenate([first * cosine - second * sine, first * sine + second * cosine], -1)
    return turned.astype(jnp.bfloat16)


def layer_norm_gain(summed, gain):
    centre = summed - jnp.mean(summed, -1, keepdims=True)
    spread = jnp.mean(centre * centre, -1, keepdims=True)
    return centre * lax.rsqrt(spread + 1e-06) * gain


MESH = pl.DeviceIdType.MESH


def flip_bits(a, b, size):
    out = 0
    bit = 1
    while bit < size:
        out = out + ((a // bit + b // bit) % 2) * bit
        bit *= 2
    return out


def at_sp(index):
    return {"sp": index}


def at_tp(index):
    return {"tp": index}


def tp_partners(n_tp):
    t = lax.axis_index("tp")
    t1 = t + 1 - 2 * (t % 2)
    t2 = (t + n_tp // 2) % n_tp
    t3 = (t1 + n_tp // 2) % n_tp
    return t, t1, t2, t3


def attn_kernel(n_sp, heads, kv_heads, width, exponent_scale, q_ref, kv_ref, o_ref, slots, m_s, l_s, acc, send, recv):
    me = lax.axis_index("sp")
    pair = me + 1 - 2 * (me % 2)
    group = heads // kv_heads

    barrier = pltpu.get_barrier_semaphore()
    pl.semaphore_signal(barrier, inc=1, device_id=at_sp(pair), device_id_type=MESH)

    def greet(j, _):
        pl.semaphore_signal(
            barrier, inc=1, device_id=at_sp(flip_bits(me, 2 * j, n_sp)), device_id_type=MESH
        )
        return 0

    lax.fori_loop(1, n_sp // 2, greet, 0)
    pl.semaphore_wait(barrier, n_sp // 2)

    def copy(src, slot, target):
        return pltpu.make_async_remote_copy(
            src_ref=src,
            dst_ref=slots.at[slot],
            send_sem=send.at[slot],
            recv_sem=recv.at[slot],
            device_id=at_sp(target),
            device_id_type=MESH,
        )

    copy(kv_ref, 1, pair).start()

    def spread(j, _):
        copy(kv_ref, 2 * j, flip_bits(me, 2 * j, n_sp)).start()
        return 0

    lax.fori_loop(1, n_sp // 2, spread, 0)

    m_s[...] = jnp.full(m_s.shape, -1e30, jnp.float32)
    l_s[...] = jnp.zeros(l_s.shape, jnp.float32)
    acc[...] = jnp.zeros(acc.shape, jnp.float32)

    def process(block):
        for h in range(heads):
            g = h // group
            q = q_ref[:, h * width : (h + 1) * width]
            k = block[:, g * width : (g + 1) * width]
            v = block[:, (kv_heads + g) * width : (kv_heads + g + 1) * width]
            s = lax.dot_general(q, k, (((1,), (1,)), ((), ())), preferred_element_type=jnp.float32)
            m_prev = m_s[h]
            m_new = jnp.maximum(m_prev, jnp.max(s, -1, keepdims=True))
            m_s[h] = m_new
            alpha = jnp.exp2((m_prev - m_new) * exponent_scale)
            p = jnp.exp2((s - m_new[:, :1]) * exponent_scale)
            l_s[h] = l_s[h] * alpha + jnp.sum(p, -1, keepdims=True)
            acc[h] = acc[h] * alpha + jnp.dot(
                p.astype(jnp.bfloat16), v, preferred_element_type=jnp.float32
            )

    process(kv_ref)

    def step(j, _):
        even = 2 * j + 2
        copy(kv_ref, even, pair).wait_recv()
        copy(slots.at[even], even + 1, pair).start()
        copy(kv_ref, even - 1, pair).wait_recv()
        process(slots.at[even - 1])
        process(slots.at[even])
        return 0

    lax.fori_loop(0, n_sp // 2 - 1, step, 0)
    copy(kv_ref, n_sp - 1, pair).wait_recv()
    process(slots.at[n_sp - 1])
    for h in range(heads):
        o_ref[:, h * width : (h + 1) * width] = (acc[h] / l_s[h]).astype(jnp.bfloat16)

    def drain(slot, _):
        copy(kv_ref, slot, pair).wait_send()
        return 0

    lax.fori_loop(1, n_sp, drain, 0)


def attend(q_rot, kv, n_sp, heads, kv_heads, width):
    rows = q_rot.shape[0]
    return pl.pallas_call(
        functools.partial(
            attn_kernel, n_sp, heads, kv_heads, width, width ** (-0.5) * 1.4426950408889634
        ),
        out_shape=jax.ShapeDtypeStruct((rows, heads * width), jnp.bfloat16),
        in_specs=[pl.BlockSpec(memory_space=pltpu.VMEM)] * 2,
        out_specs=pl.BlockSpec(memory_space=pltpu.VMEM),
        scratch_shapes=[
            pltpu.VMEM((n_sp,) + kv.shape, jnp.bfloat16),
            pltpu.VMEM((heads, rows, 128), jnp.float32),
            pltpu.VMEM((heads, rows, 128), jnp.float32),
            pltpu.VMEM((heads, rows, width), jnp.float32),
            pltpu.SemaphoreType.DMA((n_sp,)),
            pltpu.SemaphoreType.DMA((n_sp,)),
        ],
        compiler_params=pltpu.CompilerParams(collective_id=0, has_side_effects=True),
        name="attend",
    )(q_rot, kv)


def dispatch_kernel(n_sp, n_tp, out_ref, piece, stage, local, send, recv):
    me = lax.axis_index("sp")
    t, t1, t2, t3 = tp_partners(n_tp)

    barrier = pltpu.get_barrier_semaphore()
    pl.semaphore_signal(barrier, inc=1, device_id=at_tp(t1), device_id_type=MESH)
    pl.semaphore_signal(barrier, inc=1, device_id=at_tp(t2), device_id_type=MESH)

    def greet(k, _):
        pl.semaphore_signal(
            barrier, inc=1, device_id=at_sp(flip_bits(me, k, n_sp)), device_id_type=MESH
        )
        return 0

    lax.fori_loop(1, n_sp, greet, 0)
    pl.semaphore_wait(barrier, n_sp + 1)

    def copy(src, owner, source, kind, k, target):
        return pltpu.make_async_remote_copy(
            src_ref=src,
            dst_ref=piece.at[source, owner],
            send_sem=send.at[kind, k],
            recv_sem=recv.at[kind, k],
            device_id=target,
            device_id_type=MESH,
        )

    mine = out_ref.at[me]
    keep = pltpu.make_async_copy(mine, stage, local.at[0])
    keep.start()
    copy(mine, t, me, 2, 0, at_tp(t2)).start()
    copy(mine, t, me, 1, 0, at_tp(t1)).start()

    def spread(k, _):
        other = flip_bits(me, k, n_sp)
        copy(out_ref.at[other], t, me, 0, k, at_sp(other)).start()
        return 0

    lax.fori_loop(1, n_sp, spread, 0)
    keep.wait()
    put = pltpu.make_async_copy(stage, piece.at[me, t], local.at[1])
    put.start()

    def relay(k):
        source = flip_bits(me, k, n_sp)
        copy(mine, t2, source, 2, k, at_tp(t2)).wait_recv()
        copy(piece.at[source, t2], t2, source, 3, k, at_tp(t1)).start()

    def forward(k, _):
        source = flip_bits(me, k, n_sp)
        copy(mine, t, source, 0, k, at_tp(t1)).wait_recv()
        copy(piece.at[source, t], t, source, 2, k, at_tp(t2)).start()
        copy(piece.at[source, t], t, source, 1, k, at_tp(t1)).start()
        relay(k - 1)
        return 0

    lax.fori_loop(1, n_sp, forward, 0)
    relay(n_sp - 1)

    def drain(k, _):
        source = flip_bits(me, k, n_sp)
        copy(mine, t1, source, 1, k, at_tp(t1)).wait()
        copy(mine, t2, source, 2, k, at_tp(t2)).wait_send()
        copy(mine, t3, source, 3, k, at_tp(t1)).wait()
        return 0

    lax.fori_loop(0, n_sp, drain, 0)

    def drain_first(k, _):
        copy(mine, t, me, 0, k, at_tp(t1)).wait_send()
        return 0

    lax.fori_loop(1, n_sp, drain_first, 0)
    put.wait()


def dispatch(outgoing, n_sp, n_tp):
    block = outgoing.shape[1:]
    return pl.pallas_call(
        functools.partial(dispatch_kernel, n_sp, n_tp),
        out_shape=jax.ShapeDtypeStruct((n_sp, n_tp) + block, jnp.bfloat16),
        in_specs=[pl.BlockSpec(memory_space=pl.ANY)],
        out_specs=pl.BlockSpec(memory_space=pl.ANY),
        scratch_shapes=[
            pltpu.VMEM(block, jnp.bfloat16),
            pltpu.SemaphoreType.DMA((2,)),
            pltpu.SemaphoreType.DMA((4, n_sp)),
            pltpu.SemaphoreType.DMA((4, n_sp)),
        ],
        compiler_params=pltpu.CompilerParams(collective_id=1, has_side_effects=True),
        name="dispatch",
    )(outgoing)


def reduce_kernel(steps, n_tp, back, part, out, from_core, from_pair, pair_sum, total, send, recv):
    me = lax.axis_index("sp")
    t, t1, t2, t3 = tp_partners(n_tp)

    barrier = pltpu.get_barrier_semaphore()
    pl.semaphore_signal(barrier, inc=1, device_id=at_tp(t1), device_id_type=MESH)
    pl.semaphore_signal(barrier, inc=1, device_id=at_tp(t2), device_id_type=MESH)
    if back:

        def greet(k, _):
            pl.semaphore_signal(
                barrier, inc=1, device_id=at_sp(flip_bits(me, k, steps)), device_id_type=MESH
            )
            return 0

        lax.fori_loop(1, steps, greet, 0)
        pl.semaphore_wait(barrier, steps + 1)
    else:
        pl.semaphore_wait(barrier, 2)

    def order(i):
        return steps - 1 - i

    def block_of(k, lane):
        return flip_bits(me, k, steps) * n_tp + lane if back else lane * steps + k

    def copy(src, dst, kind, k, target):
        return pltpu.make_async_remote_copy(
            src_ref=src,
            dst_ref=dst,
            send_sem=send.at[kind, k],
            recv_sem=recv.at[kind, k],
            device_id=target,
            device_id_type=MESH,
        )

    def core_copy(k, half):
        lane = t3 if half else t1
        return copy(part.at[block_of(k, lane)], from_core.at[k, half], half, k, at_tp(t1))

    def pair_copy(k):
        return copy(pair_sum.at[k], from_pair.at[k], 2, k, at_tp(t2))

    def back_copy(k):
        return copy(total.at[k], out.at[me], 3, k, at_sp(flip_bits(me, k, steps)))

    def first(i, _):
        k = order(i)
        core_copy(k, 1).start()
        core_copy(k, 0).start()
        return 0

    lax.fori_loop(0, steps, first, 0)

    width = part.shape[-1]
    strip = 512 if width % 512 == 0 else width

    def add_pair(k):
        core_copy(k, 1).wait_recv()
        own = block_of(k, t2)
        for c in range(0, width, strip):
            cols = slice(c, c + strip)
            pair_sum[k, :, cols] = (
                part[own, :, cols].astype(jnp.float32)
                + from_core[k, 1, :, cols].astype(jnp.float32)
            ).astype(jnp.bfloat16)
        pair_copy(k).start()

    def add_all(k, dst, row):
        core_copy(k, 0).wait_recv()
        pair_copy(k).wait_recv()
        own = block_of(k, t)
        for c in range(0, width, strip):
            cols = slice(c, c + strip)
            dst[row, :, cols] = (
                part[own, :, cols].astype(jnp.float32)
                + from_core[k, 0, :, cols].astype(jnp.float32)
                + from_pair[k, :, cols].astype(jnp.float32)
            ).astype(jnp.bfloat16)

    def finish(k):
        if back:
            add_all(k, total, k)
            back_copy(k).start()
        else:
            add_all(k, out, k)

    depth = min(2, steps - 1)
    for i in range(depth):
        add_pair(order(i))

    def middle(i, _):
        add_pair(order(i))
        finish(order(i - depth))
        return 0

    lax.fori_loop(depth, steps, middle, 0)
    for i in range(steps - depth, steps - 1):
        finish(order(i))
    if back:
        add_all(0, out, me)
    else:
        finish(0)

    def drain(k, _):
        core_copy(k, 0).wait_send()
        core_copy(k, 1).wait_send()
        pair_copy(k).wait_send()
        return 0

    lax.fori_loop(0, steps, drain, 0)
    if back:

        def drain_back(k, _):
            back_copy(k).wait()
            return 0

        lax.fori_loop(1, steps, drain_back, 0)


def reduce_lanes(part, steps, n_tp, back, collective_id):
    block = part.shape[1:]
    slots = pltpu.VMEM((steps,) + block, jnp.bfloat16)
    return pl.pallas_call(
        functools.partial(reduce_kernel, steps, n_tp, back),
        out_shape=jax.ShapeDtypeStruct((steps,) + block, jnp.bfloat16),
        in_specs=[pl.BlockSpec(memory_space=pltpu.VMEM)],
        out_specs=pl.BlockSpec(memory_space=pltpu.VMEM),
        scratch_shapes=[
            pltpu.VMEM((steps, 2) + block, jnp.bfloat16),
            slots,
            slots,
            slots if back else pltpu.VMEM((1,) + block, jnp.bfloat16),
            pltpu.SemaphoreType.DMA((4, steps)),
            pltpu.SemaphoreType.DMA((4, steps)),
        ],
        compiler_params=pltpu.CompilerParams(collective_id=collective_id, has_side_effects=True),
        name="reduce_back" if back else "reduce_proj",
    )(part)


def per_device(
    resid,
    queries,
    keys,
    values,
    q_gain,
    key_norm_gain,
    out_weight,
    norm1_gain,
    norm2_gain,
    expert_ids,
    group_weight,
    expert_weight,
    gate_proj,
    up_proj,
    down_proj,
):
    local_tokens = queries.shape[0]
    head_size = q_gain.shape[0]
    kv_local = keys.shape[1] // head_size
    query_group = queries.shape[1] // head_size // kv_local
    model_width = resid.shape[1]
    grid_positions = lax.axis_index("sp") * local_tokens + jnp.arange(local_tokens, dtype=jnp.int32)
    q_rot = apply_rotary_heads(
        queries.reshape(local_tokens, kv_local * query_group, head_size), q_gain, grid_positions
    )
    q_rot = q_rot.reshape(local_tokens, kv_local * query_group * head_size)
    rotated_keys = apply_rotary_heads(
        keys.reshape(local_tokens, kv_local, head_size), key_norm_gain, grid_positions
    )
    rotated_keys = rotated_keys.reshape(local_tokens, kv_local * head_size)
    lanes = lax.axis_size("tp")
    sp_count = lax.axis_size("sp")
    own_rows = local_tokens // lanes
    kv = jnp.concatenate([rotated_keys, values], 1)
    attn = attend(q_rot, kv, sp_count, kv_local * query_group, kv_local, head_size)
    proj_part = jnp.dot(attn, out_weight, preferred_element_type=jnp.float32).astype(jnp.bfloat16)
    proj_rows = 16
    proj_steps = own_rows // proj_rows
    proj = reduce_lanes(
        proj_part.reshape(lanes * proj_steps, proj_rows, model_width), proj_steps, lanes, False, 2
    )
    proj = proj.reshape(own_rows, model_width)
    summed = deep_alpha * resid.astype(jnp.float32) + proj.astype(jnp.float32)
    x_one = layer_norm_gain(summed, norm1_gain).astype(jnp.bfloat16)
    top_count = expert_ids.shape[1]
    expert_local = gate_proj.shape[0]
    expert_total = expert_local * sp_count
    capacity = (3 * top_count * own_rows + 2 * expert_total - 1) // (2 * expert_total)
    flat_ids = expert_ids.reshape(-1)
    one_hot = (flat_ids[:, None] == jnp.arange(expert_total, dtype=jnp.int32)[None, :]).astype(
        jnp.int32
    )
    earlier = jnp.cumsum(one_hot, 0) - one_hot
    rank = jnp.sum(earlier * one_hot, 1)
    slot = flat_ids * capacity + rank
    placing = slot[:, None] == jnp.arange(expert_total * capacity, dtype=jnp.int32)[None, :]
    placing = placing.astype(jnp.bfloat16).reshape(own_rows, top_count, expert_total * capacity)
    placing = jnp.sum(placing, 1)
    outgoing = lax.dot_general(
        placing, x_one, (((0,), (0,)), ((), ())), preferred_element_type=jnp.float32
    ).astype(jnp.bfloat16)
    outgoing = outgoing.reshape(expert_total, capacity, model_width)
    blocks = outgoing.reshape(sp_count, expert_local * capacity, model_width)
    piece = dispatch(blocks, sp_count, lanes)
    piece = piece.reshape(sp_count * lanes, expert_local, capacity, model_width)
    gate_part = jnp.einsum("recd,edf->recf", piece, gate_proj, preferred_element_type=jnp.float32)
    up_part = jnp.einsum("recd,edf->recf", piece, up_proj, preferred_element_type=jnp.float32)
    hidden = (jax.nn.silu(gate_part) * up_part).astype(jnp.bfloat16)
    partial_sum = jnp.einsum("recf,efd->recd", hidden, down_proj, preferred_element_type=jnp.float32)
    rounded = partial_sum.astype(jnp.bfloat16)
    rounded = rounded.reshape(sp_count * lanes, expert_local * capacity, model_width)
    returned = reduce_lanes(rounded, sp_count, lanes, True, 3)
    returned = returned.reshape(expert_total * capacity, model_width)
    picked_out = returned[slot].reshape(own_rows, top_count, model_width)
    gates = group_weight[:, None] * expert_weight / jnp.sum(expert_weight, -1, keepdims=True)
    moe = jnp.sum(gates[..., None] * picked_out.astype(jnp.float32), 1)
    final = deep_alpha * x_one.astype(jnp.float32) + moe
    return layer_norm_gain(final, norm2_gain).astype(jnp.bfloat16)


def solution(mesh):
    in_specs = (
        P(("sp", "tp"), None),
        P("sp", "tp"),
        P("sp", "tp"),
        P("sp", "tp"),
        P(),
        P(),
        P("tp", None),
        P(),
        P(),
        P(("sp", "tp"), None),
        P(("sp", "tp")),
        P(("sp", "tp"), None),
        P("sp", None, "tp"),
        P("sp", None, "tp"),
        P("sp", "tp", None),
    )
    out_specs = P(("sp", "tp"), None)
    return jax.shard_map(
        per_device, mesh=mesh, in_specs=in_specs, out_specs=out_specs, check_vma=False
    )
```

time: 360 us -> 194 us (0.54)
  waiting for transfers between devices: 156 us -> 0 us
  Pallas kernels: 0 us -> 144 us
  blocking collectives: 109 us -> 0 us
  matrix products: 41.8 us -> 24.7 us
  between operations: 13.5 us -> 0.35 us
  starting transfers between devices: 9.18 us -> 0 us
  other arithmetic: 19.7 us -> 13.9 us
    pallas_call x0 -> x4, Pallas kernels: none -> 144 us  [the longest x2 69.2 us: reduce_lanes(): pl.pallas_call(functools.partial(reduce_kernel, steps, n_tp, back), out_s...]
    all_gather x2 -> x0, blocking collectives: 66.3 us -> none  [the longest x1 33.3 us: per_device(): value_piece = lax.all_gather(values, 'sp', axis=0, tiled=True)]
    reduce_scatter x1 -> x0, waiting for transfers between devices: 59 us -> none  [per_device(): lax.psum_scatter(rounded.astype(jnp.float32).astype(jnp.bfloat16), 'tp',...]
    all_gather x2 -> x0, waiting for transfers between devices: 51.1 us -> none  [the longest x1 44.4 us: per_device(): piece = lax.all_gather(arrived, 'tp', axis=0, tiled=True)]
    all_to_all x2 -> x0, waiting for transfers between devices: 44.8 us -> none  [the longest x1 36.6 us: per_device(): lax.all_to_all(returning, 'sp', split_axis=0, concat_axis=0, tiled=True)]
    all_to_all x1 -> x0, blocking collectives: 42.8 us -> none  [per_device(): lax.all_to_all(outgoing, 'sp', split_axis=0, concat_axis=0, tiled=True)]
    dot_general x11 -> x3, matrix products: 41.2 us -> 22.9 us  [the longest x1 12.8 us: per_device(): jnp.einsum('recf,efd->recd', hidden, down_proj, preferred_element_type=jn...]
    all_to_all x2 -> x0, starting transfers between devices: 8.92 us -> none  [the longest x1 5.51 us: per_device(): lax.all_to_all(returning, 'sp', split_axis=0, concat_axis=0, tiled=True)]
  transfers between devices with their start and end apart: 5 -> 0, of which waited for: 5 -> 0; matrix products, arithmetic and copies ran while one was open for 7% -> 0% of each run, Pallas kernels for 0% -> 0%
where the time goes in v1:
time: 194 us
  Pallas kernels  144 us (74%)
  matrix products  24.7 us (13%)
  other arithmetic  13.9 us (7%)
  local copies, waits for them, and re-layouts  10.9 us (6%)
    pallas_call x2, Pallas kernels, reduce_lanes(): pl.pallas_call(functools.partial(reduce_kernel, steps, n_tp, back), out_s...  69.2 us
    pallas_call x1, Pallas kernels, dispatch(): pl.pallas_call(functools.partial(dispatch_kernel, n_sp, n_tp), out_shape=...  47.4 us
    pallas_call x1, Pallas kernels, attend(): pl.pallas_call(functools.partial(attn_kernel, n_sp, heads, kv_heads, widt...  27.1 us
    dot_general x1, matrix products, per_device(): jnp.einsum('recf,efd->recd', hidden, down_proj, preferred_element_type=jn...  12.8 us
    dot_general x1, matrix products, per_device(): jnp.einsum('recd,edf->recf', piece, gate_proj, preferred_element_type=jnp...  5.22 us
    dot_general x1, matrix products, per_device(): jnp.dot(attn, out_weight, preferred_element_type=jnp.float32)  4.89 us
    gather x1, local copies, waits for them, and re-layouts, per_device(): picked_out = returned[slot].reshape(own_rows, top_count, model_width)  4.8 us
    reduce_sum x1, other arithmetic, per_device(): moe = jnp.sum(gates[..., None] * picked_out.astype(jnp.float32), 1)  4.79 us

profile of v1, /device:TPU:0, one launch (start us, length us, event | category | flops | bytes accessed | tf_op | source)
XLA Modules:
  0.0 193.5 jit_solution(5051448761658953160)
XLA Ops:
  0.2 0.5 fusion.41
  0.7 1.1 reshape.351
  1.8 0.3 multiply_reduce_fusion.3
  2.3 0.3 multiply_multiply_fusion
  2.6 0.5 subtract_convert_fusion
  3.1 0.4 pad_maximum_fusion
  3.5 0.7 copy.40
  4.5 0.6 fusion.35
  5.1 0.7 pad_maximum_fusion.3.kv_ref
  5.8 27.1 %attend.1 = bf16[256,512]{1,0:T(8,128)(2,1)} custom-call(bf16[256,512]{1,0:T(8,128)(2,1)} %bitcast.89, bf16[256,256]{1,0:T(8,128)(2,1)} %pad_maximum_fusion.3.kv_ref), custom_call_target="tpu_custom_call" | custom-call | tf_op jit(solution)/shard_map/attend/pallas_call | solution.py:151
  32.9 4.9 %convolution_convert_fusion.1 = bf16[256,4096]{1,0:T(8,128)(2,1)} fusion(bf16[256,512]{1,0:T(8,128)(2,1)} %attend.1, bf16[512,4096]{1,0:T(8,128)(2,1)} %param.21), kind=kOutput, calls=%fused_computation.2 | convolution fusion | flops 1074790400 | bytes 6553600 | tf_op jit(solution)/shard_map/dot_general | solution.py:442
  37.8 18.3 %reduce_proj.1 = bf16[4,16,4096]{2,1,0:T(8,128)(2,1)} custom-call(bf16[16,16,4096]{2,1,0:T(8,128)(2,1)} %bitcast.87), custom_call_target="tpu_custom_call" | custom-call | tf_op jit(solution)/shard_map/reduce_proj/pallas_call | solution.py:388
  56.2 1.4 fusion.22
  57.5 1.4 multiply_reduce_fusion.2
  60.3 1.7 convolution_convert_fusion.2
  62.0 47.4 %dispatch.1 = bf16[8,4,24,4096]{3,2,1,0:T(8,128)(2,1)} custom-call(bf16[8,24,4096]{2,1,0:T(8,128)(2,1)} %bitcast.86), custom_call_target="tpu_custom_call" | custom-call | tf_op jit(solution)/shard_map/dispatch/pallas_call | solution.py:249
  109.5 5.2 %fusion.5 = f32[32,1,24,256]{3,2,0,1:T(8,128)S(1)} fusion(bf16[32,24,4096]{2,1,0:T(8,128)(2,1)} %bitcast.84, bf16[1,4096,256]{2,1,0:T(8,128)(2,1)} %param.27), kind=kOutput, calls=%fused_computation.10 | convolution fusion | flops 1610612736 | bytes 9175040 | tf_op jit(solution)/shard_map/recd,edf->recf/dot_general | solution.py:472
  114.7 12.8 %convolution_convert_fusion.part = bf16[32,24,4096]{2,1,0:T(8,128)(2,1)} fusion(bf16[1,256,4096]{2,1,0:T(8,128)(2,1)S(1)} %copy-done, bf16[32,24,4096]{2,1,0:T(8,128)(2,1)} %bitcast.85, bf16[1,4096,256]{2,1,0:T(8,128)(2,1)} %param.28, f32[32,1,24,256]{3,2,0,1:T(8,128)S(1)} %fusion.5), kind=kOutput, calls=%fused_computation.1 | convolution fusion | flops 3225550848 | bytes 17563648 | tf_op jit(solution)/shard_map/recf,efd->recd/dot_general | solution.py:475
  127.5 50.9 %reduce_back.1 = bf16[8,24,4096]{2,1,0:T(8,128)(2,1)} custom-call(bf16[32,24,4096]{2,1,0:T(8,128)(2,1)} %convolution_convert_fusion.part), custom_call_target="tpu_custom_call" | custom-call | tf_op jit(solution)/shard_map/reduce_back/pallas_call | solution.py:388
  178.6 4.8 %gather_fusion = bf16[128,4096]{1,0:T(8,128)(2,1)} fusion(bf16[192,4096]{1,0:T(8,128)(2,1)} %bitcast.83, s32[1024]{0:T(1024)S(1)} %pad_clamp_fusion), kind=kCustom, calls=%fused_computation | custom fusion | bytes 2097664 | tf_op jit(solution)/shard_map/gather | solution.py:480
  183.4 3.4 %reshape.353 = f32[64,2,4096]{2,1,0:T(2,128)} reshape(bf16[128,4096]{1,0:T(8,128)(2,1)} %gather_fusion) | data formatting | bytes 3145728 | tf_op jit(solution)/shard_map/convert_element_type | solution.py:482
  187.0 4.8 %multiply_reduce_fusion = f32[64,4096]{1,0:T(8,128)S(1)} fusion(f32[64,2,4096]{2,1,0:T(2,128)} %reshape.353, f32[64,2]{1,0:T(8,128)S(1)} %copy.33), kind=kLoop, calls=%fused_computation.9 | loop fusion | flops 786432 | bytes 3146240 | tf_op jit(solution)/shard_map/reduce_sum | solution.py:482
  192.1 0.3 multiply_reduce_fusion.1
  192.5 1.0 multiply_convert_fusion
  (52 shorter events, 2.4 us)
Async XLA Ops:
  0.0 114.7 %copy-start = (bf16[1,256,4096]{2,1,0:T(8,128)(2,1)S(1)}, bf16[1,256,4096]{2,1,0:T(8,128)(2,1)}, u32[]{:S(2)}) copy-start(bf16[1,256,4096]{2,1,0:T(8,128)(2,1)} %param.29) | copy-start | bytes 6291460
  0.0 2.2 %copy-start.9 = (f32[128]{0:T(128)S(1)}, f32[128]{0:T(128)}, u32[]{:S(2)}) copy-start(f32[128]{0:T(128)} %param.19) | copy-start | bytes 1540
  2.2 2.0 %copy-start.3 = (bf16[256,128]{1,0:T(8,128)(2,1)S(1)}, bf16[256,128]{1,0:T(8,128)(2,1)}, u32[]{:S(2)}) copy-start(bf16[256,128]{1,0:T(8,128)(2,1)} %param.17) | copy-start | bytes 196612
  2.2 2.1 %copy-start.10 = (f32[128]{0:T(128)S(1)}, f32[128]{0:T(128)}, u32[]{:S(2)}) copy-start(f32[128]{0:T(128)} %param.20) | copy-start | bytes 1540
  2.6 2.5 %copy-start.4 = (bf16[256,128]{1,0:T(8,128)(2,1)S(1)}, bf16[256,128]{1,0:T(8,128)(2,1)}, u32[]{:S(2)}) copy-start(bf16[256,128]{1,0:T(8,128)(2,1)} %param.18) | copy-start | bytes 196612
  37.8 18.3 %copy-start.2 = (bf16[64,4096]{1,0:T(8,128)(2,1)S(1)}, bf16[64,4096]{1,0:T(8,128)(2,1)}, u32[]{:S(2)}) copy-start(bf16[64,4096]{1,0:T(8,128)(2,1)} %param.15) | copy-start | bytes 1572868
  37.8 21.1 %copy-start.5 = (f32[4096]{0:T(1024)S(1)}, f32[4096]{0:T(1024)}, u32[]{:S(2)}) copy-start(f32[4096]{0:T(1024)} %param.22) | copy-start | bytes 49156
  56.1 2.8 %copy-start.1 = (bf16[4,16,4096]{2,1,0:T(8,128)(2,1)S(1)}, bf16[4,16,4096]{2,1,0:T(8,128)(2,1)}, u32[]{:S(2)}) copy-start(bf16[4,16,4096]{2,1,0:T(8,128)(2,1)} %reduce_proj.1) | copy-start | bytes 1572868
  56.1 3.1 %copy-start.8 = (s32[64,2]{0,1:T(2,128)S(1)}, s32[64,2]{0,1:T(2,128)}, u32[]{:S(2)}) copy-start(s32[64,2]{0,1:T(2,128)} %param.24) | copy-start | bytes 1540
  183.4 3.4 %copy-start.7 = (f32[64,2]{0,1:T(2,128)S(1)}, f32[64,2]{0,1:T(2,128)}, u32[]{:S(2)}) copy-start(f32[64,2]{0,1:T(2,128)} %param.26) | copy-start | bytes 1540
  183.4 3.4 %copy-start.11 = (f32[64]{0:T(128)S(1)}, f32[64]{0:T(128)}, u32[]{:S(2)}) copy-start(f32[64]{0:T(128)} %param.25) | copy-start | bytes 772
  191.8 0.7 copy-start.6

commit v2 on v1

--- a/solution.py
+++ b/solution.py
@@ -168,9 +168,42 @@
     )(q_rot, kv)
 
 
-def dispatch_kernel(n_sp, n_tp, out_ref, piece, stage, local, send, recv):
+def moe_kernel(
+    n_sp,
+    n_tp,
+    stride,
+    out_ref,
+    gate_hbm,
+    up_hbm,
+    down_hbm,
+    back,
+    w_gate,
+    w_up,
+    w_down,
+    piece,
+    rows,
+    part,
+    from_core,
+    from_pair,
+    pair_sum,
+    total,
+    local,
+    send,
+    recv,
+):
     me = lax.axis_index("sp")
     t, t1, t2, t3 = tp_partners(n_tp)
+    cap, width = out_ref.shape[1:]
+    strip = 1024 if width % 1024 == 0 else width
+
+    loads = [
+        pltpu.make_async_copy(src, dst, local.at[i])
+        for i, (src, dst) in enumerate(
+            ((gate_hbm, w_gate), (up_hbm, w_up), (down_hbm, w_down), (out_ref.at[me], piece.at[me, t]))
+        )
+    ]
+    for load in loads:
+        load.start()
 
     barrier = pltpu.get_barrier_semaphore()
     pl.semaphore_signal(barrier, inc=1, device_id=at_tp(t1), device_id_type=MESH)
@@ -185,81 +218,192 @@
     lax.fori_loop(1, n_sp, greet, 0)
     pl.semaphore_wait(barrier, n_sp + 1)
 
-    def copy(src, owner, source, kind, k, target):
+    def order(i):
+        return jnp.where(i < 2, i, 2 + (i - 2 + n_sp // 2 - 2) % max(n_sp - 2, 1))
+
+    def copy(src, dst, kind, k, target):
         return pltpu.make_async_remote_copy(
             src_ref=src,
-            dst_ref=piece.at[source, owner],
+            dst_ref=dst,
             send_sem=send.at[kind, k],
             recv_sem=recv.at[kind, k],
             device_id=target,
             device_id_type=MESH,
         )
 
-    mine = out_ref.at[me]
-    keep = pltpu.make_async_copy(mine, stage, local.at[0])
-    keep.start()
-    copy(mine, t, me, 2, 0, at_tp(t2)).start()
-    copy(mine, t, me, 1, 0, at_tp(t1)).start()
-
-    def spread(k, _):
-        other = flip_bits(me, k, n_sp)
-        copy(out_ref.at[other], t, me, 0, k, at_sp(other)).start()
+    def owner(k):
+        return flip_bits(me, k, n_sp)
+
+    def first_copy(k):
+        return copy(out_ref.at[owner(k)], piece.at[me, t], 0, k, at_sp(owner(k)))
+
+    def core_forward(k):
+        return copy(piece.at[owner(k), t], piece.at[owner(k), t], 1, k, at_tp(t1))
+
+    def pair_forward(k):
+        return copy(piece.at[owner(k), t], piece.at[owner(k), t], 2, k, at_tp(t2))
+
+    def relay_copy(k):
+        return copy(piece.at[owner(k), t2], piece.at[owner(k), t2], 3, k, at_tp(t1))
+
+    def core_part(k, half):
+        lane = t3 if half else t1
+        return copy(part.at[k, lane], from_core.at[k, half], 4 + half, k, at_tp(t1))
+
+    def pair_part(k):
+        return copy(pair_sum.at[k], from_pair.at[k], 6, k, at_tp(t2))
+
+    def back_copy(k):
+        return copy(total.at[k], back.at[me], 7, k, at_sp(owner(k)))
+
+    copy(out_ref.at[me], piece.at[me, t], 2, 0, at_tp(t2)).start()
+    copy(out_ref.at[me], piece.at[me, t], 1, 0, at_tp(t1)).start()
+
+    def spread(i, _):
+        first_copy(order(i)).start()
         return 0
 
     lax.fori_loop(1, n_sp, spread, 0)
-    keep.wait()
-    put = pltpu.make_async_copy(stage, piece.at[me, t], local.at[1])
-    put.start()
-
-    def relay(k):
-        source = flip_bits(me, k, n_sp)
-        copy(mine, t2, source, 2, k, at_tp(t2)).wait_recv()
-        copy(piece.at[source, t2], t2, source, 3, k, at_tp(t1)).start()
-
-    def forward(k, _):
-        source = flip_bits(me, k, n_sp)
-        copy(mine, t, source, 0, k, at_tp(t1)).wait_recv()
-        copy(piece.at[source, t], t, source, 2, k, at_tp(t2)).start()
-        copy(piece.at[source, t], t, source, 1, k, at_tp(t1)).start()
-        relay(k - 1)
-        return 0
-
-    lax.fori_loop(1, n_sp, forward, 0)
-    relay(n_sp - 1)
+    rows[...] = jnp.zeros(rows.shape, jnp.float32)
+    for load in loads:
+        load.wait()
+
+    def stage_forward(k):
+        first_copy(k).wait_recv()
+        pair_forward(k).start()
+        core_forward(k).start()
+
+    def stage_relay(k):
+        pair_forward(k).wait_recv()
+        relay_copy(k).start()
+
+    def stage_expert(k):
+        core_forward(k).wait_recv()
+        relay_copy(k).wait_recv()
+        source = owner(k)
+        for lane in range(n_tp):
+            rows[lane * stride : lane * stride + cap, :] = piece[source, lane].astype(jnp.float32)
+        gate = jnp.zeros((n_tp * stride, w_gate.shape[1]), jnp.float32)
+        up = jnp.zeros((n_tp * stride, w_up.shape[1]), jnp.float32)
+        for c in range(0, width, strip):
+            x = rows[:, c : c + strip].astype(jnp.bfloat16)
+            gate += jnp.dot(x, w_gate[c : c + strip, :], preferred_element_type=jnp.float32)
+            up += jnp.dot(x, w_up[c : c + strip, :], preferred_element_type=jnp.float32)
+        hidden = (gate / (1.0 + jnp.exp(-gate)) * up).astype(jnp.bfloat16)
+        for c in range(0, width, strip):
+            y = jnp.dot(hidden, w_down[:, c : c + strip], preferred_element_type=jnp.float32)
+            for lane in range(n_tp):
+                part[k, lane, :, c : c + strip] = y[lane * stride : lane * stride + cap].astype(
+                    jnp.bfloat16
+                )
+        core_part(k, 1).start()
+        core_part(k, 0).start()
+
+    def stage_pair(k):
+        core_part(k, 1).wait_recv()
+        for c in range(0, width, strip):
+            cols = slice(c, c + strip)
+            pair_sum[k, :, cols] = (
+                part[k, t2, :, cols].astype(jnp.float32)
+                + from_core[k, 1, :, cols].astype(jnp.float32)
+            ).astype(jnp.bfloat16)
+        pair_part(k).start()
+
+    def stage_total(k):
+        core_part(k, 0).wait_recv()
+        pair_part(k).wait_recv()
+
+        def add(dst, row):
+            for c in range(0, width, strip):
+                cols = slice(c, c + strip)
+                dst[row, :, cols] = (
+                    part[k, t, :, cols].astype(jnp.float32)
+                    + from_core[k, 0, :, cols].astype(jnp.float32)
+                    + from_pair[k, :, cols].astype(jnp.float32)
+                ).astype(jnp.bfloat16)
+
+        @pl.when(k == 0)
+        def _():
+            add(back, me)
+
+        @pl.when(k > 0)
+        def _():
+            add(total, k)
+            back_copy(k).start()
+
+    def tick(i, _):
+        @pl.when(jnp.logical_and(i >= 1, i < n_sp))
+        def _():
+            stage_forward(order(i))
+
+        @pl.when(jnp.logical_and(i >= 1, i < n_sp + 1))
+        def _():
+            stage_relay(order(i - 1))
+
+        @pl.when(jnp.logical_and(i >= 2, i < n_sp + 2))
+        def _():
+            stage_expert(order(i - 2))
+
+        @pl.when(jnp.logical_and(i >= 3, i < n_sp + 3))
+        def _():
+            stage_pair(order(i - 3))
+
+        @pl.when(i >= 4)
+        def _():
+            stage_total(order(i - 4))
+
+        return 0
+
+    lax.fori_loop(0, n_sp + 4, tick, 0)
 
     def drain(k, _):
-        source = flip_bits(me, k, n_sp)
-        copy(mine, t1, source, 1, k, at_tp(t1)).wait()
-        copy(mine, t2, source, 2, k, at_tp(t2)).wait_send()
-        copy(mine, t3, source, 3, k, at_tp(t1)).wait()
+        core_forward(k).wait_send()
+        pair_forward(k).wait_send()
+        relay_copy(k).wait_send()
+        core_part(k, 0).wait_send()
+        core_part(k, 1).wait_send()
+        pair_part(k).wait_send()
         return 0
 
     lax.fori_loop(0, n_sp, drain, 0)
 
-    def drain_first(k, _):
-        copy(mine, t, me, 0, k, at_tp(t1)).wait_send()
-        return 0
-
-    lax.fori_loop(1, n_sp, drain_first, 0)
-    put.wait()
-
-
-def dispatch(outgoing, n_sp, n_tp):
+    def drain_far(k, _):
+        first_copy(k).wait_send()
+        back_copy(k).wait()
+        return 0
+
+    lax.fori_loop(1, n_sp, drain_far, 0)
+
+
+def experts(outgoing, gate_proj, up_proj, down_proj, n_sp, n_tp):
     block = outgoing.shape[1:]
+    stride = (block[0] + 7) // 8 * 8
+    slots = pltpu.VMEM((n_sp,) + block, jnp.bfloat16)
+    lanes = pltpu.VMEM((n_sp, n_tp) + block, jnp.bfloat16)
+    anywhere = pl.BlockSpec(memory_space=pl.ANY)
     return pl.pallas_call(
-        functools.partial(dispatch_kernel, n_sp, n_tp),
-        out_shape=jax.ShapeDtypeStruct((n_sp, n_tp) + block, jnp.bfloat16),
-        in_specs=[pl.BlockSpec(memory_space=pl.ANY)],
-        out_specs=pl.BlockSpec(memory_space=pl.ANY),
+        functools.partial(moe_kernel, n_sp, n_tp, stride),
+        out_shape=jax.ShapeDtypeStruct(outgoing.shape, jnp.bfloat16),
+        in_specs=[pl.BlockSpec(memory_space=pltpu.VMEM), anywhere, anywhere, anywhere],
+        out_specs=pl.BlockSpec(memory_space=pltpu.VMEM),
         scratch_shapes=[
-            pltpu.VMEM(block, jnp.bfloat16),
-            pltpu.SemaphoreType.DMA((2,)),
-            pltpu.SemaphoreType.DMA((4, n_sp)),
-            pltpu.SemaphoreType.DMA((4, n_sp)),
+            pltpu.VMEM(gate_proj.shape, jnp.bfloat16),
+            pltpu.VMEM(up_proj.shape, jnp.bfloat16),
+            pltpu.VMEM(down_proj.shape, jnp.bfloat16),
+            lanes,
+            pltpu.VMEM((n_tp * stride, block[1]), jnp.float32),
+            lanes,
+            pltpu.VMEM((n_sp, 2) + block, jnp.bfloat16),
+            slots,
+            slots,
+            slots,
+            pltpu.SemaphoreType.DMA((4,)),
+            pltpu.SemaphoreType.DMA((8, n_sp)),
+            pltpu.SemaphoreType.DMA((8, n_sp)),
         ],
         compiler_params=pltpu.CompilerParams(collective_id=1, has_side_effects=True),
-        name="dispatch",
-    )(outgoing)
+        name="experts",
+    )(outgoing, gate_proj, up_proj, down_proj)
 
 
 def reduce_kernel(steps, n_tp, back, part, out, from_core, from_pair, pair_sum, total, send, recv):
@@ -459,27 +603,29 @@
     earlier = jnp.cumsum(one_hot, 0) - one_hot
     rank = jnp.sum(earlier * one_hot, 1)
     slot = flat_ids * capacity + rank
-    placing = slot[:, None] == jnp.arange(expert_total * capacity, dtype=jnp.int32)[None, :]
-    placing = placing.astype(jnp.bfloat16).reshape(own_rows, top_count, expert_total * capacity)
-    placing = jnp.sum(placing, 1)
+    chosen = slot[:, None] == jnp.arange(expert_total * capacity, dtype=jnp.int32)[None, :]
+    chosen = chosen.reshape(own_rows, top_count, expert_total * capacity)
+    placing = jnp.sum(chosen.astype(jnp.bfloat16), 1)
     outgoing = lax.dot_general(
         placing, x_one, (((0,), (0,)), ((), ())), preferred_element_type=jnp.float32
     ).astype(jnp.bfloat16)
     outgoing = outgoing.reshape(expert_total, capacity, model_width)
     blocks = outgoing.reshape(sp_count, expert_local * capacity, model_width)
-    piece = dispatch(blocks, sp_count, lanes)
-    piece = piece.reshape(sp_count * lanes, expert_local, capacity, model_width)
-    gate_part = jnp.einsum("recd,edf->recf", piece, gate_proj, preferred_element_type=jnp.float32)
-    up_part = jnp.einsum("recd,edf->recf", piece, up_proj, preferred_element_type=jnp.float32)
-    hidden = (jax.nn.silu(gate_part) * up_part).astype(jnp.bfloat16)
-    partial_sum = jnp.einsum("recf,efd->recd", hidden, down_proj, preferred_element_type=jnp.float32)
-    rounded = partial_sum.astype(jnp.bfloat16)
-    rounded = rounded.reshape(sp_count * lanes, expert_local * capacity, model_width)
-    returned = reduce_lanes(rounded, sp_count, lanes, True, 3)
+    returned = experts(
+        blocks,
+        gate_proj.reshape(gate_proj.shape[1:]),
+        up_proj.reshape(up_proj.shape[1:]),
+        down_proj.reshape(down_proj.shape[1:]),
+        sp_count,
+        lanes,
+    )
     returned = returned.reshape(expert_total * capacity, model_width)
-    picked_out = returned[slot].reshape(own_rows, top_count, model_width)
     gates = group_weight[:, None] * expert_weight / jnp.sum(expert_weight, -1, keepdims=True)
-    moe = jnp.sum(gates[..., None] * picked_out.astype(jnp.float32), 1)
+    combine = jnp.sum(jnp.where(chosen, gates[..., None], 0.0), 1)
+    high = lax.reduce_precision(combine, 8, 7)
+    both = jnp.concatenate([high, combine - high], 0).astype(jnp.bfloat16)
+    picked = jnp.dot(both, returned, preferred_element_type=jnp.float32)
+    moe = picked[:own_rows] + picked[own_rows:]
     final = deep_alpha * x_one.astype(jnp.float32) + moe
     return layer_norm_gain(final, norm2_gain).astype(jnp.bfloat16)
 

time: 194 us -> 168 us (0.87)
  matrix products: 24.7 us -> 8.47 us
  local copies, waits for them, and re-layouts: 10.9 us -> 2.18 us
    pallas_call x2 -> x1, Pallas kernels: 69.2 us -> 18.3 us  [reduce_lanes(): pl.pallas_call(functools.partial(reduce_kernel, steps, n_tp, back), out_s...]
    pallas_call x1, Pallas kernels: 47.4 us -> 97.9 us  [experts(): pl.pallas_call(functools.partial(moe_kernel, n_sp, n_tp, stride), out_sha...]
    dot_general x2 -> x1, matrix products: 18 us -> 1.84 us  [per_device(): picked = jnp.dot(both, returned, preferred_element_type=jnp.float32)]
    gather x1 -> x0, local copies, waits for them, and re-layouts: 4.8 us -> none  [per_device(): picked_out = returned[slot].reshape(own_rows, top_count, model_width)]
    reduce_sum x2, other arithmetic: 4.89 us -> 0.19 us  [the longest x1 0.1 us: per_device(): combine = jnp.sum(jnp.where(chosen, gates[..., None], 0.0), 1)]
    convert_element_type x1 -> x0, local copies, waits for them, and re-layouts: 3.42 us -> none  [per_device(): moe = jnp.sum(gates[..., None] * picked_out.astype(jnp.float32), 1)]
where the time goes in v2:
time: 168 us; the launch traced here: 167 us
  Pallas kernels  143 us (85%)
  other arithmetic  12.9 us (8%)
  matrix products  8.47 us (5%)
  local copies, waits for them, and re-layouts  2.18 us (1%)
    pallas_call x1, Pallas kernels, experts(): pl.pallas_call(functools.partial(moe_kernel, n_sp, n_tp, stride), out_sha...  97.9 us
    pallas_call x1, Pallas kernels, attend(): pl.pallas_call(functools.partial(attn_kernel, n_sp, heads, kv_heads, widt...  27.1 us
    pallas_call x1, Pallas kernels, reduce_lanes(): pl.pallas_call(functools.partial(reduce_kernel, steps, n_tp, back), out_s...  18.3 us
    dot_general x1, matrix products, per_device(): jnp.dot(attn, out_weight, preferred_element_type=jnp.float32)  4.89 us

profile of v2, /device:TPU:0, one launch (start us, length us, event | category | flops | bytes accessed | tf_op | source)
XLA Modules:
  0.0 167.2 jit_solution(2232908930468754862)
XLA Ops:
  0.0 0.7 reduce_sum.101
  0.7 0.7 multiply_divide_fusion
  1.4 1.0 fusion.2
  2.4 0.8 copy.33
  4.0 0.7 multiply_add_fusion
  4.9 0.9 fusion.4
  6.0 0.6 fusion.7
  6.6 0.7 pad_maximum_fusion.3.kv_ref
  7.4 0.5 fusion.18
  8.1 0.3 multiply_reduce_fusion.2
  8.5 0.3 multiply_multiply_fusion
  8.9 0.5 subtract_convert_fusion
  9.4 0.4 pad_maximum_fusion
  9.8 0.7 copy.38
  10.5 27.1 %attend.1 = bf16[256,512]{1,0:T(8,128)(2,1)} custom-call(bf16[256,512]{1,0:T(8,128)(2,1)} %bitcast.37, bf16[256,256]{1,0:T(8,128)(2,1)} %pad_maximum_fusion.3.kv_ref), custom_call_target="tpu_custom_call" | custom-call | tf_op jit(solution)/shard_map/attend/pallas_call | solution.py:151
  37.6 4.9 %convolution_convert_fusion = bf16[256,4096]{1,0:T(8,128)(2,1)} fusion(bf16[256,512]{1,0:T(8,128)(2,1)} %attend.1, bf16[512,4096]{1,0:T(8,128)(2,1)} %param.21), kind=kOutput, calls=%fused_computation | convolution fusion | flops 1074790400 | bytes 6553600 | tf_op jit(solution)/shard_map/dot_general | solution.py:586
  42.5 18.3 %reduce_proj.1 = bf16[4,16,4096]{2,1,0:T(8,128)(2,1)} custom-call(bf16[16,16,4096]{2,1,0:T(8,128)(2,1)} %bitcast.32), custom_call_target="tpu_custom_call" | custom-call | tf_op jit(solution)/shard_map/reduce_proj/pallas_call | solution.py:532
  60.8 1.4 fusion.1
  62.2 1.4 multiply_reduce_fusion.1
  63.6 0.3 multiply_convert_fusion.1
  63.9 1.7 %convolution_convert_fusion.1 = bf16[192,4096]{1,0:T(8,128)(2,1)} fusion(bf16[64,192]{1,0:T(8,128)(2,1)S(1)} %fusion.9, bf16[64,4096]{1,0:T(8,128)(2,1)S(1)} %multiply_convert_fusion.1), kind=kOutput, calls=%fused_computation.1 | convolution fusion | flops 101449728 | bytes 2121728 | tf_op jit(solution)/shard_map/dot_general | solution.py:609
  65.7 97.9 %experts.1 = bf16[8,24,4096]{2,1,0:T(8,128)(2,1)} custom-call(bf16[8,24,4096]{2,1,0:T(8,128)(2,1)} %bitcast.31, bf16[4096,256]{1,0:T(8,128)(2,1)} %bitcast.33, bf16[4096,256]{1,0:T(8,128)(2,1)} %bitcast.34, bf16[256,4096]{1,0:T(8,128)(2,1)} %bitcast.35), custom_call_target="tpu_custom_call" | custom-call | tf_op jit(solution)/shard_map/experts/pallas_call | solution.py:384
  163.6 1.8 %fusion.10 = f32[128,4096]{1,0:T(8,128)S(1)} fusion(bf16[192,4096]{1,0:T(8,128)(2,1)} %bitcast.30, bf16[64,192]{1,0:T(8,128)(2,1)S(1)} %get-tuple-element.14, bf16[64,192]{1,0:T(8,128)(2,1)S(1)} %get-tuple-element.13), kind=kOutput, calls=%fused_computation.36 | convolution fusion | flops 201424896 | bytes 3719168 | tf_op jit(solution)/shard_map/dot_general | solution.py:627
  166.2 1.0 multiply_convert_fusion
  (35 shorter events, 2.1 us)
Async XLA Ops:
  0.0 6.6 %copy-start.3 = (bf16[256,128]{1,0:T(8,128)(2,1)S(1)}, bf16[256,128]{1,0:T(8,128)(2,1)}, u32[]{:S(2)}) copy-start(bf16[256,128]{1,0:T(8,128)(2,1)} %param.18) | copy-start | bytes 196612
  0.0 7.9 %copy-start.2 = (bf16[256,512]{1,0:T(8,128)(2,1)S(1)}, bf16[256,512]{1,0:T(8,128)(2,1)}, u32[]{:S(2)}) copy-start(bf16[256,512]{1,0:T(8,128)(2,1)} %param.16) | copy-start | bytes 786436
  4.0 4.5 %copy-start.6 = (f32[128]{0:T(128)S(1)}, f32[128]{0:T(128)}, u32[]{:S(2)}) copy-start(f32[128]{0:T(128)} %param.19) | copy-start | bytes 1540
  42.5 18.3 %copy-start.1 = (bf16[64,4096]{1,0:T(8,128)(2,1)S(1)}, bf16[64,4096]{1,0:T(8,128)(2,1)}, u32[]{:S(2)}) copy-start(bf16[64,4096]{1,0:T(8,128)(2,1)} %param.15) | copy-start | bytes 1572868
  42.5 21.1 %copy-start.4 = (f32[4096]{0:T(1024)S(1)}, f32[4096]{0:T(1024)}, u32[]{:S(2)}) copy-start(f32[4096]{0:T(1024)} %param.22) | copy-start | bytes 49156
  60.8 2.8 %copy-start = (bf16[4,16,4096]{2,1,0:T(8,128)(2,1)S(1)}, bf16[4,16,4096]{2,1,0:T(8,128)(2,1)}, u32[]{:S(2)}) copy-start(bf16[4,16,4096]{2,1,0:T(8,128)(2,1)} %reduce_proj.1) | copy-start | bytes 1572868
  165.5 0.7 copy-start.5

commit v3 on v2

--- a/solution.py
+++ b/solution.py
@@ -66,10 +66,12 @@
     return t, t1, t2, t3
 
 
-def attn_kernel(n_sp, heads, kv_heads, width, exponent_scale, q_ref, kv_ref, o_ref, slots, m_s, l_s, acc, send, recv):
+def attn_kernel(n_sp, heads, kv_heads, width, exponent_scale, q_ref, kv_ref, w_hbm, o_ref, slots, m_s, l_s, acc, attn, w, local, send, recv):
     me = lax.axis_index("sp")
     pair = me + 1 - 2 * (me % 2)
     group = heads // kv_heads
+    load = pltpu.make_async_copy(w_hbm, w, local.at[0])
+    load.start()
 
     barrier = pltpu.get_barrier_semaphore()
     pl.semaphore_signal(barrier, inc=1, device_id=at_sp(pair), device_id_type=MESH)
@@ -137,7 +139,14 @@
     copy(kv_ref, n_sp - 1, pair).wait_recv()
     process(slots.at[n_sp - 1])
     for h in range(heads):
-        o_ref[:, h * width : (h + 1) * width] = (acc[h] / l_s[h]).astype(jnp.bfloat16)
+        attn[:, h * width : (h + 1) * width] = (acc[h] / l_s[h]).astype(jnp.bfloat16)
+    load.wait()
+    columns = w.shape[1]
+    strip = 512 if columns % 512 == 0 else columns
+    for c in range(0, columns, strip):
+        o_ref[:, c : c + strip] = jnp.dot(
+            attn[...], w[:, c : c + strip], preferred_element_type=jnp.float32
+        ).astype(jnp.bfloat16)
 
     def drain(slot, _):
         copy(kv_ref, slot, pair).wait_send()
@@ -146,26 +155,29 @@
     lax.fori_loop(1, n_sp, drain, 0)
 
 
-def attend(q_rot, kv, n_sp, heads, kv_heads, width):
+def attend(q_rot, kv, out_weight, n_sp, heads, kv_heads, width):
     rows = q_rot.shape[0]
     return pl.pallas_call(
         functools.partial(
             attn_kernel, n_sp, heads, kv_heads, width, width ** (-0.5) * 1.4426950408889634
         ),
-        out_shape=jax.ShapeDtypeStruct((rows, heads * width), jnp.bfloat16),
-        in_specs=[pl.BlockSpec(memory_space=pltpu.VMEM)] * 2,
+        out_shape=jax.ShapeDtypeStruct((rows, out_weight.shape[1]), jnp.bfloat16),
+        in_specs=[pl.BlockSpec(memory_space=pltpu.VMEM)] * 2 + [pl.BlockSpec(memory_space=pl.ANY)],
         out_specs=pl.BlockSpec(memory_space=pltpu.VMEM),
         scratch_shapes=[
             pltpu.VMEM((n_sp,) + kv.shape, jnp.bfloat16),
             pltpu.VMEM((heads, rows, 128), jnp.float32),
             pltpu.VMEM((heads, rows, 128), jnp.float32),
             pltpu.VMEM((heads, rows, width), jnp.float32),
+            pltpu.VMEM((rows, heads * width), jnp.bfloat16),
+            pltpu.VMEM(out_weight.shape, jnp.bfloat16),
+            pltpu.SemaphoreType.DMA((1,)),
             pltpu.SemaphoreType.DMA((n_sp,)),
             pltpu.SemaphoreType.DMA((n_sp,)),
         ],
         compiler_params=pltpu.CompilerParams(collective_id=0, has_side_effects=True),
         name="attend",
-    )(q_rot, kv)
+    )(q_rot, kv, out_weight)
 
 
 def moe_kernel(
@@ -342,19 +354,19 @@
 
         @pl.when(jnp.logical_and(i >= 2, i < n_sp + 2))
         def _():
-            stage_expert(order(i - 2))
-
-        @pl.when(jnp.logical_and(i >= 3, i < n_sp + 3))
+            stage_pair(order(i - 2))
+
+        @pl.when(i >= 3)
         def _():
-            stage_pair(order(i - 3))
-
-        @pl.when(i >= 4)
+            stage_total(order(i - 3))
+
+        @pl.when(jnp.logical_and(i >= 1, i < n_sp + 1))
         def _():
-            stage_total(order(i - 4))
-
-        return 0
-
-    lax.fori_loop(0, n_sp + 4, tick, 0)
+            stage_expert(order(i - 1))
+
+        return 0
+
+    lax.fori_loop(0, n_sp + 3, tick, 0)
 
     def drain(k, _):
         core_forward(k).wait_send()
@@ -582,8 +594,9 @@
     sp_count = lax.axis_size("sp")
     own_rows = local_tokens // lanes
     kv = jnp.concatenate([rotated_keys, values], 1)
-    attn = attend(q_rot, kv, sp_count, kv_local * query_group, kv_local, head_size)
-    proj_part = jnp.dot(attn, out_weight, preferred_element_type=jnp.float32).astype(jnp.bfloat16)
+    proj_part = attend(
+        q_rot, kv, out_weight, sp_count, kv_local * query_group, kv_local, head_size
+    )
     proj_rows = 16
     proj_steps = own_rows // proj_rows
     proj = reduce_lanes(

time: 168 us -> 163 us (0.970)
  matrix products: 8.47 us -> 3.58 us
    dot_general x1 -> x0, matrix products: 4.89 us -> none  [per_device(): jnp.dot(attn, out_weight, preferred_element_type=jnp.float32)]
    pallas_call x1, Pallas kernels: 97.9 us -> 95.8 us  [experts(): pl.pallas_call(functools.partial(moe_kernel, n_sp, n_tp, stride), out_sha...]
    pallas_call x1, Pallas kernels: 27.1 us -> 29 us  [attend(): pl.pallas_call(functools.partial(attn_kernel, n_sp, heads, kv_heads, widt...]
where the time goes in v3:
time: 163 us; the launch traced here: 162 us
  Pallas kernels  143 us (88%)
  other arithmetic  13 us (8%)
  matrix products  3.58 us (2%)
  local copies, waits for them, and re-layouts  2.14 us (1%)
    pallas_call x1, Pallas kernels, experts(): pl.pallas_call(functools.partial(moe_kernel, n_sp, n_tp, stride), out_sha...  95.8 us
    pallas_call x1, Pallas kernels, attend(): pl.pallas_call(functools.partial(attn_kernel, n_sp, heads, kv_heads, widt...  29 us
    pallas_call x1, Pallas kernels, reduce_lanes(): pl.pallas_call(functools.partial(reduce_kernel, steps, n_tp, back), out_s...  18.3 us

profile of v3, /device:TPU:0, one launch (start us, length us, event | category | flops | bytes accessed | tf_op | source)
XLA Modules:
  0.0 162.0 jit_solution(10921172110403608962)
XLA Ops:
  0.0 0.7 reduce_sum.101
  0.7 0.7 multiply_divide_fusion
  1.4 1.0 fusion.2
  2.4 0.8 copy.33
  4.0 0.7 multiply_add_fusion
  4.9 0.9 fusion.4
  6.0 0.6 fusion.7
  6.6 0.8 pad_maximum_fusion.3.kv_ref
  7.4 0.5 fusion.18
  8.1 0.3 multiply_reduce_fusion.2
  8.5 0.3 multiply_multiply_fusion
  8.9 0.5 subtract_convert_fusion
  9.4 0.4 pad_maximum_fusion
  9.7 0.7 copy.38
  10.5 29.0 %attend.1 = bf16[256,4096]{1,0:T(8,128)(2,1)} custom-call(bf16[256,512]{1,0:T(8,128)(2,1)} %bitcast.35, bf16[256,256]{1,0:T(8,128)(2,1)} %pad_maximum_fusion.3.kv_ref, bf16[512,4096]{1,0:T(8,128)(2,1)} %w_hbm.1), custom_call_target="tpu_custom_call" | custom-call | tf_op jit(solution)/shard_map/attend/pallas_call | solution.py:160
  39.5 18.3 %reduce_proj.1 = bf16[4,16,4096]{2,1,0:T(8,128)(2,1)} custom-call(bf16[16,16,4096]{2,1,0:T(8,128)(2,1)} %bitcast.28), custom_call_target="tpu_custom_call" | custom-call | tf_op jit(solution)/shard_map/reduce_proj/pallas_call | solution.py:544
  57.8 1.4 fusion.1
  59.2 1.4 multiply_reduce_fusion.1
  60.7 0.3 multiply_convert_fusion.1
  61.0 1.7 %convolution_convert_fusion = bf16[192,4096]{1,0:T(8,128)(2,1)} fusion(bf16[64,192]{1,0:T(8,128)(2,1)S(1)} %fusion.9, bf16[64,4096]{1,0:T(8,128)(2,1)S(1)} %multiply_convert_fusion.1), kind=kOutput, calls=%fused_computation | convolution fusion | flops 101449728 | bytes 2121728 | tf_op jit(solution)/shard_map/dot_general | solution.py:622
  62.7 95.8 %experts.1 = bf16[8,24,4096]{2,1,0:T(8,128)(2,1)} custom-call(bf16[8,24,4096]{2,1,0:T(8,128)(2,1)} %bitcast.30, bf16[4096,256]{1,0:T(8,128)(2,1)} %bitcast.31, bf16[4096,256]{1,0:T(8,128)(2,1)} %bitcast.32, bf16[256,4096]{1,0:T(8,128)(2,1)} %bitcast.33), custom_call_target="tpu_custom_call" | custom-call | tf_op jit(solution)/shard_map/experts/pallas_call | solution.py:396
  158.5 1.8 %fusion.10 = f32[128,4096]{1,0:T(8,128)S(1)} fusion(bf16[192,4096]{1,0:T(8,128)(2,1)} %bitcast.29, bf16[64,192]{1,0:T(8,128)(2,1)S(1)} %get-tuple-element.14, bf16[64,192]{1,0:T(8,128)(2,1)S(1)} %get-tuple-element.13), kind=kOutput, calls=%fused_computation.35 | convolution fusion | flops 201424896 | bytes 3719168 | tf_op jit(solution)/shard_map/dot_general | solution.py:640
  160.3 0.3 fusion.25
  161.0 1.0 multiply_convert_fusion
  (34 shorter events, 1.8 us)
Async XLA Ops:
  0.0 6.6 %copy-start.3 = (bf16[256,128]{1,0:T(8,128)(2,1)S(1)}, bf16[256,128]{1,0:T(8,128)(2,1)}, u32[]{:S(2)}) copy-start(bf16[256,128]{1,0:T(8,128)(2,1)} %param.18) | copy-start | bytes 196612
  0.0 7.9 %copy-start.2 = (bf16[256,512]{1,0:T(8,128)(2,1)S(1)}, bf16[256,512]{1,0:T(8,128)(2,1)}, u32[]{:S(2)}) copy-start(bf16[256,512]{1,0:T(8,128)(2,1)} %param.16) | copy-start | bytes 786436
  4.0 4.5 %copy-start.6 = (f32[128]{0:T(128)S(1)}, f32[128]{0:T(128)}, u32[]{:S(2)}) copy-start(f32[128]{0:T(128)} %param.19) | copy-start | bytes 1540
  39.5 18.3 %copy-start.1 = (bf16[64,4096]{1,0:T(8,128)(2,1)S(1)}, bf16[64,4096]{1,0:T(8,128)(2,1)}, u32[]{:S(2)}) copy-start(bf16[64,4096]{1,0:T(8,128)(2,1)} %param.15) | copy-start | bytes 1572868
  39.5 21.1 %copy-start.4 = (f32[4096]{0:T(1024)S(1)}, f32[4096]{0:T(1024)}, u32[]{:S(2)}) copy-start(f32[4096]{0:T(1024)} %param.22) | copy-start | bytes 49156
  57.8 2.8 %copy-start = (bf16[4,16,4096]{2,1,0:T(8,128)(2,1)S(1)}, bf16[4,16,4096]{2,1,0:T(8,128)(2,1)}, u32[]{:S(2)}) copy-start(bf16[4,16,4096]{2,1,0:T(8,128)(2,1)} %reduce_proj.1) | copy-start | bytes 1572868
  160.3 0.7 copy-start.5
